TPU v7x, 32 devices: a whole 2x2x4 slice. The times are simulated.
32 devices in a mesh: grp: 2 (over y), sp: 4 (over z), tp: 4 (over x, core).
Axes of the slice: x: 2, y: 2, z: 4, core: 2. Of those that a mesh axis runs over, the one named last changes fastest.
Arguments:
- residual: bfloat16 [2048, 2048], P(('grp', 'sp')), parts along dimension 0, may hold values from -6 to 6
- queries: bfloat16 [2048, 1024], P(('grp', 'sp'), 'tp'), parts along dimension 0, may hold values from -400 to 400
- keys: bfloat16 [2048, 1024], P(('grp', 'sp'), 'tp'), parts along dimension 0, may hold values from -8 to 8
- values: bfloat16 [2048, 1024], P(('grp', 'sp'), 'tp'), parts along dimension 0, may hold values from -6 to 6
- log_gates: float32 [2048, 16], P(('grp', 'sp'), 'tp'), parts along dimension 0, may hold values from -126 to 0, as said below
- w_out: bfloat16 [1024, 2048], P('tp'), may hold values from -0.75 to 0.75
- norm_gain: float32 [2048], replicated, may hold values from 0.1 to 1.9
- w_gate: bfloat16 [2048, 5632], P('sp', 'tp'), may hold values from -0.125 to 0.125
- w_up: bfloat16 [2048, 5632], P('sp', 'tp'), may hold values from -0.125 to 0.125
- w_down: bfloat16 [5632, 2048], P('tp', 'sp'), may hold values from -0.078125 to 0.078125
Outputs:
- output: bfloat16 [2048, 2048], P(('grp', 'sp', 'tp')), parts along dimension 0
There are 2 independent parts, one for each index of `grp`. A program takes and returns all parts, laid end to end along the dimension named above; an argument that names none is the same for every part. Nothing has to cross between parts.
Inputs may be any that keep to these rules, and one draw needn't show every extreme that they name: `log_gates`: never rises along positions.
All inputs are finite; a program needn't handle non-finite values.
Results may differ from a plain program's by a relative error of at most 0.014.
Values may be sent and summed in bfloat16 or wider, within the bound.
A program may use at most 128 MiB of HBM per device.

v0:
```python
import math
import jax
import jax.numpy as jnp
from jax import lax
from jax.sharding import PartitionSpec as P


def normalize(rows_in, gain):
    floats = rows_in.astype(jnp.float32)
    scaled = floats * lax.rsqrt(jnp.mean(floats * floats, axis=-1, keepdims=True) + 1e-06)
    return (scaled * gain).astype(jnp.bfloat16)


def attend(queries, keys, values, log_gates):
    row_count = queries.shape[0]
    head_count = log_gates.shape[1]
    head_width = queries.shape[1] // head_count
    score_scale = head_width ** (-0.5)
    first_row = lax.axis_index("sp") * row_count
    query_heads = queries.reshape(row_count, head_count, head_width)
    query_gates = log_gates.T
    query_positions = first_row + jnp.arange(row_count, dtype=jnp.int32)
    initial = (
        jnp.full((head_count, row_count), -1e30, jnp.float32),
        jnp.zeros((head_count, row_count), jnp.float32),
        jnp.zeros((head_count, row_count, head_width), jnp.float32),
    )
    carried = initial
    key_piece = lax.all_gather(keys.astype(jnp.float32), "sp", axis=0, tiled=True).astype(
        jnp.bfloat16
    )
    value_piece = lax.all_gather(values.astype(jnp.float32), "sp", axis=0, tiled=True).astype(
        jnp.bfloat16
    )
    gate_piece = lax.all_gather(log_gates, "sp", axis=0, tiled=True)
    length = key_piece.shape[0]
    block_rows = math.gcd(length, 2048)
    block_count = length // block_rows
    key_blocks = key_piece.reshape(block_count, block_rows, head_count, head_width)
    value_blocks = value_piece.reshape(block_count, block_rows, head_count, head_width)
    gate_blocks = gate_piece.reshape(block_count, block_rows, head_count)
    offsets = jnp.arange(block_count, dtype=jnp.int32) * block_rows

    def one_block(state, inputs):
        current_key_block, value_block, gate_block, offset = inputs

        def work(current):
            running_max, running_sum, accumulated = current
            scores = (
                jnp.einsum(
                    "qhd,khd->hqk",
                    query_heads,
                    current_key_block,
                    preferred_element_type=jnp.float32,
                )
                * score_scale
            )
            scores = scores + query_gates[:, :, None] - gate_block.T[:, None, :]
            key_positions = offset + jnp.arange(block_rows, dtype=jnp.int32)
            causal = (query_positions[:, None] >= key_positions[None, :])[None]
            scores = jnp.where(causal, scores, -1e30)
            new_max = jnp.maximum(running_max, jnp.max(scores, axis=-1))
            weights = jnp.where(causal, jnp.exp(scores - new_max[:, :, None]), 0.0)
            rescale = jnp.exp(running_max - new_max)
            running_sum = running_sum * rescale + jnp.sum(weights, axis=-1)
            product = jnp.einsum(
                "hqk,khd->hqd",
                weights.astype(jnp.bfloat16),
                value_block,
                preferred_element_type=jnp.float32,
            )
            accumulated = accumulated * rescale[:, :, None] + product
            return (new_max, running_sum, accumulated)

        state = lax.cond(offset <= first_row + row_count - 1, work, lambda current: current, state)
        return (state, None)

    carried, _ = lax.scan(one_block, carried, (key_blocks, value_blocks, gate_blocks, offsets))
    running_max, running_sum, accumulated = carried
    attended = accumulated / running_sum[:, :, None]
    return (
        attended.transpose(1, 0, 2).reshape(row_count, head_count * head_width).astype(jnp.bfloat16)
    )


def body(residual, queries, keys, values, log_gates, w_out, norm_gain, w_gate, w_up, w_down):
    attended = attend(queries, keys, values, log_gates)
    row_count = attended.shape[0]
    per_device = row_count // lax.axis_size("tp")
    my_first = lax.axis_index("tp") * per_device
    projected = lax.psum(
        jnp.dot(attended, w_out, preferred_element_type=jnp.float32).astype(jnp.bfloat16), "tp"
    ).astype(jnp.float32)
    mixed_all = (residual.astype(jnp.float32) + projected).astype(jnp.bfloat16)
    normed_all = normalize(mixed_all, norm_gain)
    mixed = lax.dynamic_slice_in_dim(mixed_all, my_first, per_device, 0)
    gate_whole = lax.all_gather(w_gate, "sp", axis=0, tiled=True)
    up_whole = lax.all_gather(w_up, "sp", axis=0, tiled=True)
    down_whole = lax.all_gather(w_down, "sp", axis=1, tiled=True)
    gate_proj = jnp.dot(normed_all, gate_whole, preferred_element_type=jnp.float32)
    up_proj = jnp.dot(normed_all, up_whole, preferred_element_type=jnp.float32)
    hidden = (jax.nn.silu(gate_proj) * up_proj).astype(jnp.bfloat16)
    down_sum = lax.psum_scatter(
        jnp.dot(hidden, down_whole, preferred_element_type=jnp.float32).astype(jnp.bfloat16),
        "tp",
        scatter_dimension=0,
        tiled=True,
    ).astype(jnp.float32)
    summed = mixed.astype(jnp.float32) + 0.5 * down_sum
    scaled = summed * lax.rsqrt(jnp.mean(summed * summed, axis=-1, keepdims=True) + 1e-06)
    return scaled.astype(jnp.bfloat16)


def solution(mesh):
    in_specs = (
        P(("grp", "sp"), None),
        P(("grp", "sp"), "tp"),
        P(("grp", "sp"), "tp"),
        P(("grp", "sp"), "tp"),
        P(("grp", "sp"), "tp"),
        P("tp", None),
        P(),
        P("sp", "tp"),
        P("sp", "tp"),
        P("tp", "sp"),
    )
    out_specs = P(("grp", "sp", "tp"), None)
    return jax.shard_map(body, mesh=mesh, in_specs=in_specs, out_specs=out_specs, check_vma=False)
```

profile of v0, /device:TPU:0, one launch (start us, length us, event | category | flops | bytes accessed | tf_op | source)
XLA Modules:
  0.0 429.7 jit_solution(2206887288210929115)
XLA Ops:
  7.4 0.0 copy-start
  7.4 0.0 all-reduce.2.cloned.1.call-start
  7.4 1.1 copy.12
  8.5 17.4 %all_gather.18 = bf16[1024,256]{0,1:T(8,128)(2,1)S(1)} all-gather(bf16[256,256]{0,1:T(8,128)(2,1)S(1)} %copy.12), channel_id=1, replica_groups=mesh['grp'=2,'sp'=4,'tp'=4] {'sp'}, dimensions={0}, use_global_device_ids=true | all-gather | bytes 655360 | tf_op jit(solution)/shard_map/all_gather | solution.py:29
  25.8 1.0 copy.13
  26.9 16.3 %all_gather.20 = bf16[1024,256]{0,1:T(8,128)(2,1)S(1)} all-gather(bf16[256,256]{0,1:T(8,128)(2,1)S(1)} %copy.13), channel_id=1, replica_groups=mesh['grp'=2,'sp'=4,'tp'=4] {'sp'}, dimensions={0}, use_global_device_ids=true | all-gather | bytes 655360 | tf_op jit(solution)/shard_map/all_gather | solution.py:32
  43.1 13.3 %all_gather.19 = f32[1024,4]{0,1:T(4,128)S(1)} all-gather(f32[256,4]{0,1:T(4,128)} %param.16), channel_id=1, replica_groups=mesh['grp'=2,'sp'=4,'tp'=4] {'sp'}, dimensions={0}, use_global_device_ids=true | all-gather | bytes 20480 | tf_op jit(solution)/shard_map/all_gather | solution.py:35
  56.5 7.0 %conditional.1 = ((f32[4,256]{1,0:T(4,128)S(1)}, f32[4,256,64]{1,2,0:T(8,128)S(1)})) conditional(s32[]{:T(128)} %convert_element_type.64, (f32[4,256]{1,0:T(4,128)S(1)}, f32[4,256,64]{1,2,0:T(8,128)S(1)}) %tuple.22, (s32[]{:T(128)}, s32[256]{0:T(256)S(1)}, bf16[256,256]{1,0:T(8,128)(2,1)}, bf16[1024,256]{0,1:T(8,128)(2,1)S(1)}, f32[4,256]{1,0:T(4,128)}, ...), branch_computations={%region_0.1_spmd, %region_1.0_spmd} | conditional | flops 288754944 | bytes 15727672 | solution.py:75
  56.5 0.0 copy-start.2
  56.6 0.2 iota_compare_fusion
  56.8 1.0 copy.14
  57.8 2.1 fusion.2
  59.9 0.0 copy-done.2
  59.9 2.0 fusion.1
  61.9 1.6 fusion.6
  63.5 0.0 copy-start.1
  63.6 0.0 copy-done
  63.6 1.4 convolution_convert_fusion
  65.0 0.0 copy-start.3
  65.0 0.0 all-reduce.2.cloned.1.call-update
  65.0 0.0 all-gather.4.cloned.1.call-start
  65.1 0.5 all-gather.4.cloned.1.call-update
  65.6 0.0 all-gather.6.cloned.1.call-start
  65.7 0.5 all-gather.6.cloned.1.call-update
  66.2 0.0 all-gather.8.cloned.1.call-start
  66.3 0.5 all-gather.8.cloned.1.call-update
  66.8 0.0 reduce-scatter.2.cloned.1.call-start
  66.8 35.4 %all-reduce.2.cloned.1.call-done = bf16[256,2048]{1,0:T(8,128)(2,1)} async-done(((bf16[256,2048]{1,0:T(8,128)(2,1)}), bf16[256,2048]{1,0:T(8,128)(2,1)}) %all-reduce.2.cloned.1.call-update) | async-done | bytes 1048592 | tf_op jit(solution)/shard_map/psum | solution.py:91
  102.2 0.0 copy-done.1
  102.2 1.7 fusion.13
  104.0 70.1 %all-gather.4.cloned.1.call-done = bf16[2048,1408]{1,0:T(8,128)(2,1)} async-done(((bf16[512,1408]{1,0:T(8,128)(2,1)}), bf16[2048,1408]{1,0:T(8,128)(2,1)}) %all-gather.4.cloned.1.call-update) | async-done | bytes 5767184 | tf_op jit(solution)/shard_map/all_gather | solution.py:97
  174.1 0.0 copy-done.3
  174.1 5.6 %fusion.18 = f32[256,1408]{1,0:T(8,128)} fusion(bf16[2048,1408]{1,0:T(8,128)(2,1)} %all-gather.4.cloned.1.call-done, bf16[256,2048]{1,0:T(8,128)(2,1)S(1)} %get-tuple-element.132, f32[2048]{0:T(1024)S(1)} %copy-done.3, f32[256]{0:T(256)S(1)} %add_rsqrt_fusion), kind=kOutput, calls=%fused_computation.29 | convolution fusion | flops 1478492160 | bytes 8266752 | tf_op jit(solution)/shard_map/dot_general | solution.py:100
  179.8 100.6 %all-gather.6.cloned.1.call-done = bf16[2048,1408]{1,0:T(8,128)(2,1)} async-done(((bf16[512,1408]{1,0:T(8,128)(2,1)}), bf16[2048,1408]{1,0:T(8,128)(2,1)}) %all-gather.6.cloned.1.call-update) | async-done | bytes 5767184 | tf_op jit(solution)/shard_map/all_gather | solution.py:98
  280.4 106.3 %all-gather.8.cloned.1.call-done = bf16[1408,2048]{1,0:T(8,128)(2,1)} async-done(((bf16[1408,512]{1,0:T(8,128)(2,1)}), bf16[1408,2048]{1,0:T(8,128)(2,1)}) %all-gather.8.cloned.1.call-update) | async-done | bytes 5767184 | tf_op jit(solution)/shard_map/all_gather | solution.py:99
  386.7 9.3 %convolution_convert_fusion.1 = bf16[256,2048]{1,0:T(8,128)(2,1)} fusion(bf16[1408,2048]{1,0:T(8,128)(2,1)} %all-gather.8.cloned.1.call-done, bf16[2048,1408]{1,0:T(8,128)(2,1)} %all-gather.6.cloned.1.call-done, f32[256,1408]{1,0:T(8,128)} %fusion.18, bf16[256,2048]{1,0:T(8,128)(2,1)S(1)} %get-tuple-element.132, f32[2048]{0:T(1024)S(1)} %copy-done.3, ...), kind=kOutput, calls=%fused_computation.21 | convolution fusion | flops 2957574144 | bytes 15082496 | tf_op jit(solution)/shard_map/dot_general | solution.py:104
  395.9 0.0 reduce-scatter.2.cloned.1.call-update
  396.0 23.2 %reduce-scatter.2.cloned.1.call-done = bf16[64,2048]{1,0:T(8,128)(2,1)} async-done(((bf16[256,2048]{1,0:T(8,128)(2,1)}), bf16[64,2048]{1,0:T(8,128)(2,1)}) %reduce-scatter.2.cloned.1.call-update) | async-done | bytes 262160 | tf_op jit(solution)/shard_map/reduce_scatter | solution.py:103
  419.2 1.2 multiply_reduce_fusion
  420.4 1.8 multiply_convert_fusion
  (9 shorter events, 0.1 us)
Async XLA Ops:
  7.4 56.2 %copy-start = (bf16[256,2048]{1,0:T(8,128)(2,1)S(1)}, bf16[256,2048]{1,0:T(8,128)(2,1)}, u32[]{:S(2)}) copy-start(bf16[256,2048]{1,0:T(8,128)(2,1)} %param.17) | copy-start | bytes 3145732
  7.4 94.9 %all-reduce.2.cloned.1.call-start = ((), (), s32[]{:S(2)}) async-start(), calls=%async_computation.1 | async-start | bytes 2097152 | tf_op jit(solution)/shard_map/psum | solution.py:91
  56.5 3.3 copy-start.2
  63.5 38.7 %copy-start.1 = (bf16[256,2048]{1,0:T(8,128)(2,1)S(1)}, bf16[256,2048]{1,0:T(8,128)(2,1)}, u32[]{:S(2)}) copy-start(bf16[256,2048]{1,0:T(8,128)(2,1)} %param.12) | copy-start | bytes 3145732
  65.0 109.1 %copy-start.3 = (f32[2048]{0:T(1024)S(1)}, f32[2048]{0:T(1024)}, u32[]{:S(2)}) copy-start(f32[2048]{0:T(1024)} %param.18) | copy-start | bytes 24580
  65.0 109.1 %all-gather.4.cloned.1.call-start = ((), (), s32[]{:S(2)}) async-start(), calls=%async_computation.2 | async-start | bytes 7208960 | tf_op jit(solution)/shard_map/all_gather | solution.py:97
  65.6 214.8 %all-gather.6.cloned.1.call-start = ((), (), s32[]{:S(2)}) async-start(), calls=%async_computation.3 | async-start | bytes 7208960 | tf_op jit(solution)/shard_map/all_gather | solution.py:98
  66.2 320.5 %all-gather.8.cloned.1.call-start = ((), (), s32[]{:S(2)}) async-start(), calls=%async_computation.4 | async-start | bytes 7208960 | tf_op jit(solution)/shard_map/all_gather | solution.py:99
  66.8 352.4 %reduce-scatter.2.cloned.1.call-start = ((), (), s32[]{:S(2)}) async-start(), calls=%async_computation.5 | async-start | bytes 1310720 | tf_op jit(solution)/shard_map/reduce_scatter | solution.py:103
Sparse Core Ops, SparseCore 0:
  65.2 37.0 all-reduce.1
  396.1 23.0 reduce-scatter.1
Sparse Core Ops, SparseCore 1:
  67.1 107.0 all-gather.3
  175.6 104.8 all-gather.5
  281.9 104.8 all-gather.7
where the time goes:
time: 430 us
  waiting for transfers between devices  337 us (78%)
  blocking collectives  47 us (11%)
  matrix products  20 us (5%)
  between operations  15.1 us (4%)
  other arithmetic  6.94 us (2%)
    all_gather x1, waiting for transfers between devices, body(): down_whole = lax.all_gather(w_down, 'sp', axis=1, tiled=True)  106 us
    all_gather x1, waiting for transfers between devices, body(): up_whole = lax.all_gather(w_up, 'sp', axis=0, tiled=True)  101 us
    all_gather x1, waiting for transfers between devices, body(): gate_whole = lax.all_gather(w_gate, 'sp', axis=0, tiled=True)  70.1 us
    psum x1, waiting for transfers between devices, body(): lax.psum(jnp.dot(attended, w_out, preferred_element_type=jnp.float32).ast...  35.4 us
    reduce_scatter x1, waiting for transfers between devices, body(): lax.psum_scatter(jnp.dot(hidden, down_whole, preferred_element_type=jnp.f...  23.2 us
    all_gather x1, blocking collectives, attend(): lax.all_gather(keys.astype(jnp.float32), 'sp', axis=0, tiled=True)  17.4 us
    all_gather x1, blocking collectives, attend(): lax.all_gather(values.astype(jnp.float32), 'sp', axis=0, tiled=True)  16.3 us
    all_gather x1, blocking collectives, attend(): gate_piece = lax.all_gather(log_gates, 'sp', axis=0, tiled=True)  13.3 us
  transfers between devices with their start and end apart: 5, of which 5 were waited for; matrix products, arithmetic and copies ran while one was open for 2% of the time, Pallas kernels for 0%

commit v1 on v0

--- a/solution.py
+++ b/solution.py
@@ -3,6 +3,11 @@
 import jax.numpy as jnp
 from jax import lax
 from jax.sharding import PartitionSpec as P
+
+
+def summed_here(array, axis):
+    parts = lax.all_gather(array, axis)
+    return jnp.sum(parts, axis=0)
 
 
 def normalize(rows_in, gain):
@@ -88,7 +93,7 @@
     row_count = attended.shape[0]
     per_device = row_count // lax.axis_size("tp")
     my_first = lax.axis_index("tp") * per_device
-    projected = lax.psum(
+    projected = summed_here(
         jnp.dot(attended, w_out, preferred_element_type=jnp.float32).astype(jnp.bfloat16), "tp"
     ).astype(jnp.float32)
     mixed_all = (residual.astype(jnp.float32) + projected).astype(jnp.bfloat16)

time: 430 us -> 463 us (1.077)
  waiting for transfers between devices: 337 us -> 369 us
    psum x1 -> x0, waiting for transfers between devices: 35.4 us -> none  [body(): lax.psum(jnp.dot(attended, w_out, preferred_element_type=jnp.float32).ast...]
    all_gather x1, waiting for transfers between devices: 70.1 us -> 103 us  [body(): gate_whole = lax.all_gather(w_gate, 'sp', axis=0, tiled=True)]
    all_gather x0 -> x1, waiting for transfers between devices: none -> 33 us  [summed_here(): parts = lax.all_gather(array, axis)]
    all_gather x1, waiting for transfers between devices: 101 us -> 106 us  [body(): up_whole = lax.all_gather(w_up, 'sp', axis=0, tiled=True)]
    all_gather x1, waiting for transfers between devices: 106 us -> 101 us  [body(): down_whole = lax.all_gather(w_down, 'sp', axis=1, tiled=True)]
where the time goes in v1:
time: 463 us
  waiting for transfers between devices  369 us (80%)
  blocking collectives  47 us (10%)
  matrix products  20.1 us (4%)
  between operations  13.2 us (3%)
  other arithmetic  10.1 us (2%)
    all_gather x1, waiting for transfers between devices, body(): up_whole = lax.all_gather(w_up, 'sp', axis=0, tiled=True)  106 us
    all_gather x1, waiting for transfers between devices, body(): gate_whole = lax.all_gather(w_gate, 'sp', axis=0, tiled=True)  103 us
    all_gather x1, waiting for transfers between devices, body(): down_whole = lax.all_gather(w_down, 'sp', axis=1, tiled=True)  101 us
    all_gather x1, waiting for transfers between devices, summed_here(): parts = lax.all_gather(array, axis)  33 us
    reduce_scatter x1, waiting for transfers between devices, body(): lax.psum_scatter(jnp.dot(hidden, down_whole, preferred_element_type=jnp.f...  23.2 us
    all_gather x1, blocking collectives, attend(): lax.all_gather(keys.astype(jnp.float32), 'sp', axis=0, tiled=True)  17.4 us
    all_gather x1, blocking collectives, attend(): lax.all_gather(values.astype(jnp.float32), 'sp', axis=0, tiled=True)  16.3 us
    all_gather x1, blocking collectives, attend(): gate_piece = lax.all_gather(log_gates, 'sp', axis=0, tiled=True)  13.3 us
  transfers between devices with their start and end apart: 5, of which 5 were waited for; matrix products, arithmetic and copies ran while one was open for 2% of the time, Pallas kernels for 0%

profile of v1, /device:TPU:0, one launch (start us, length us, event | category | flops | bytes accessed | tf_op | source)
XLA Modules:
  0.0 462.6 jit_solution(7669819110823955109)
XLA Ops:
  6.5 0.0 copy-start
  6.5 0.0 all-gather.12.cloned.1.call-start
  6.5 1.1 copy.12
  7.6 17.4 %all_gather.24 = bf16[1024,256]{0,1:T(8,128)(2,1)S(1)} all-gather(bf16[256,256]{0,1:T(8,128)(2,1)S(1)} %copy.12), channel_id=1, replica_groups=mesh['grp'=2,'sp'=4,'tp'=4] {'sp'}, dimensions={0}, use_global_device_ids=true | all-gather | bytes 655360 | tf_op jit(solution)/shard_map/all_gather | solution.py:34
  25.0 1.0 copy.13
  26.0 16.3 %all_gather.26 = bf16[1024,256]{0,1:T(8,128)(2,1)S(1)} all-gather(bf16[256,256]{0,1:T(8,128)(2,1)S(1)} %copy.13), channel_id=1, replica_groups=mesh['grp'=2,'sp'=4,'tp'=4] {'sp'}, dimensions={0}, use_global_device_ids=true | all-gather | bytes 655360 | tf_op jit(solution)/shard_map/all_gather | solution.py:37
  42.3 13.3 %all_gather.25 = f32[1024,4]{0,1:T(4,128)S(1)} all-gather(f32[256,4]{0,1:T(4,128)} %param.16), channel_id=1, replica_groups=mesh['grp'=2,'sp'=4,'tp'=4] {'sp'}, dimensions={0}, use_global_device_ids=true | all-gather | bytes 20480 | tf_op jit(solution)/shard_map/all_gather | solution.py:40
  55.7 7.1 %conditional.1 = ((f32[4,256]{1,0:T(4,128)S(1)}, f32[4,256,64]{1,2,0:T(8,128)S(1)})) conditional(s32[]{:T(128)} %convert_element_type.66, (f32[4,256]{1,0:T(4,128)S(1)}, f32[4,256,64]{1,2,0:T(8,128)S(1)}) %tuple.22, (s32[]{:T(128)}, s32[256]{0:T(256)S(1)}, bf16[256,256]{1,0:T(8,128)(2,1)}, bf16[1024,256]{0,1:T(8,128)(2,1)S(1)}, f32[4,256]{1,0:T(4,128)}, ...), branch_computations={%region_0.1_spmd, %region_1.0_spmd} | conditional | flops 288754944 | bytes 15727672 | solution.py:80
  55.7 0.0 copy-start.1
  55.7 0.2 iota_compare_fusion
  56.0 1.0 copy.14
  57.0 2.1 fusion.2
  59.0 0.0 copy-done.1
  59.1 2.0 fusion.1
  61.1 1.6 fusion.6
  62.8 0.0 copy-done
  62.8 1.5 convolution_convert_fusion
  64.3 0.0 all-gather.12.cloned.1.call-update
  64.3 0.0 all-gather.6.cloned.1.call-start
  64.4 0.7 all-gather.6.cloned.1.call-update
  65.1 0.0 all-gather.10.cloned.1.call-start
  65.1 0.7 all-gather.10.cloned.1.call-update
  65.8 0.0 all-gather.8.cloned.1.call-start
  65.8 0.5 all-gather.8.cloned.1.call-update
  66.4 0.0 reduce-scatter.2.cloned.1.call-start
  66.4 33.0 %all-gather.12.cloned.1.call-done = bf16[1024,2048]{1,0:T(8,128)(2,1)} async-done(((bf16[256,2048]{1,0:T(8,128)(2,1)}), bf16[1024,2048]{1,0:T(8,128)(2,1)}) %all-gather.12.cloned.1.call-update) | async-done | bytes 4194320 | tf_op jit(solution)/shard_map/all_gather | solution.py:9
  99.4 0.0 copy-start.2
  99.4 3.1 reduce_sum.41
  102.5 1.7 fusion.13
  104.2 103.5 %all-gather.6.cloned.1.call-done = bf16[2048,1408]{1,0:T(8,128)(2,1)} async-done(((bf16[512,1408]{1,0:T(8,128)(2,1)}), bf16[2048,1408]{1,0:T(8,128)(2,1)}) %all-gather.6.cloned.1.call-update) | async-done | bytes 5767184 | tf_op jit(solution)/shard_map/all_gather | solution.py:102
  207.7 0.0 copy-done.2
  207.7 5.7 %fusion.18 = f32[256,1408]{1,0:T(8,128)} fusion(bf16[2048,1408]{1,0:T(8,128)(2,1)} %all-gather.6.cloned.1.call-done, bf16[256,2048]{1,0:T(8,128)(2,1)S(1)} %get-tuple-element.132, f32[2048]{0:T(1024)S(1)} %copy-done.2, f32[256]{0:T(256)S(1)} %add_rsqrt_fusion), kind=kOutput, calls=%fused_computation.29 | convolution fusion | flops 1478492160 | bytes 8266752 | tf_op jit(solution)/shard_map/dot_general | solution.py:105
  213.3 100.9 %all-gather.10.cloned.1.call-done = bf16[1408,2048]{1,0:T(8,128)(2,1)} async-done(((bf16[1408,512]{1,0:T(8,128)(2,1)}), bf16[1408,2048]{1,0:T(8,128)(2,1)}) %all-gather.10.cloned.1.call-update) | async-done | bytes 5767184 | tf_op jit(solution)/shard_map/all_gather | solution.py:104
  314.2 106.4 %all-gather.8.cloned.1.call-done = bf16[2048,1408]{1,0:T(8,128)(2,1)} async-done(((bf16[512,1408]{1,0:T(8,128)(2,1)}), bf16[2048,1408]{1,0:T(8,128)(2,1)}) %all-gather.8.cloned.1.call-update) | async-done | bytes 5767184 | tf_op jit(solution)/shard_map/all_gather | solution.py:103
  420.6 9.3 %convolution_convert_fusion.1 = bf16[256,2048]{1,0:T(8,128)(2,1)} fusion(bf16[1408,2048]{1,0:T(8,128)(2,1)} %all-gather.10.cloned.1.call-done, bf16[2048,1408]{1,0:T(8,128)(2,1)} %all-gather.8.cloned.1.call-done, f32[256,1408]{1,0:T(8,128)} %fusion.18, bf16[256,2048]{1,0:T(8,128)(2,1)S(1)} %get-tuple-element.132, f32[2048]{0:T(1024)S(1)} %copy-done.2, ...), kind=kOutput, calls=%fused_computation.21 | convolution fusion | flops 2957574144 | bytes 15082496 | tf_op jit(solution)/shard_map/dot_general | solution.py:109
  429.9 0.0 reduce-scatter.2.cloned.1.call-update
  429.9 23.2 %reduce-scatter.2.cloned.1.call-done = bf16[64,2048]{1,0:T(8,128)(2,1)} async-done(((bf16[256,2048]{1,0:T(8,128)(2,1)}), bf16[64,2048]{1,0:T(8,128)(2,1)}) %reduce-scatter.2.cloned.1.call-update) | async-done | bytes 262160 | tf_op jit(solution)/shard_map/reduce_scatter | solution.py:108
  453.1 1.2 multiply_reduce_fusion
  454.3 1.8 multiply_convert_fusion
  (9 shorter events, 0.1 us)
Async XLA Ops:
  6.5 56.3 %copy-start = (bf16[256,2048]{1,0:T(8,128)(2,1)S(1)}, bf16[256,2048]{1,0:T(8,128)(2,1)}, u32[]{:S(2)}) copy-start(bf16[256,2048]{1,0:T(8,128)(2,1)} %param.17) | copy-start | bytes 3145732
  6.5 92.8 %all-gather.12.cloned.1.call-start = ((), (), s32[]{:S(2)}) async-start(), calls=%async_computation.5 | async-start | bytes 5242880 | tf_op jit(solution)/shard_map/all_gather | solution.py:9
  55.7 3.3 copy-start.1
  64.3 143.4 %all-gather.6.cloned.1.call-start = ((), (), s32[]{:S(2)}) async-start(), calls=%async_computation.1 | async-start | bytes 7208960 | tf_op jit(solution)/shard_map/all_gather | solution.py:102
  65.1 249.2 %all-gather.10.cloned.1.call-start = ((), (), s32[]{:S(2)}) async-start(), calls=%async_computation.3 | async-start | bytes 7208960 | tf_op jit(solution)/shard_map/all_gather | solution.py:104
  65.8 354.8 %all-gather.8.cloned.1.call-start = ((), (), s32[]{:S(2)}) async-start(), calls=%async_computation.2 | async-start | bytes 7208960 | tf_op jit(solution)/shard_map/all_gather | solution.py:103
  66.4 386.7 %reduce-scatter.2.cloned.1.call-start = ((), (), s32[]{:S(2)}) async-start(), calls=%async_computation.4 | async-start | bytes 1310720 | tf_op jit(solution)/shard_map/reduce_scatter | solution.py:108
  99.4 108.3 %copy-start.2 = (f32[2048]{0:T(1024)S(1)}, f32[2048]{0:T(1024)}, u32[]{:S(2)}) copy-start(f32[2048]{0:T(1024)} %param.18) | copy-start | bytes 24580
Sparse Core Ops, SparseCore 0:
  64.4 34.8 all-gather.11
  100.9 106.6 all-gather.5
  209.2 104.9 all-gather.9
  315.6 104.9 all-gather.7
  430.0 23.0 reduce-scatter.1
